TPU v7x, 512 devices: a whole 4x4x16 slice. The times are simulated.
512 devices in a mesh: ep: 128 (over z, x, core), tp: 4 (over y).
Axes of the slice: x: 4, y: 4, z: 16, core: 2. Of those that a mesh axis runs over, the one named last changes fastest.
Arguments:
- hidden: bfloat16 [512, 2048], P('ep'), may hold values from -6 to 6
- attn_gain: float32 [2048], replicated, may hold values from 0.3 to 3
- query_weight: bfloat16 [2048, 2048], P('ep', 'tp'), may hold values from -0.125 to 0.125
- head_bias: float32 [16], replicated, may hold values from -10 to -4
- key_cache: bfloat16 [512, 4, 1024, 128], P('ep', 'tp'), may hold values from -6 to 6
- value_cache: bfloat16 [512, 4, 1024, 128], P('ep', 'tp'), may hold values from -7 to 7
- lengths: int32 [512], P('ep'), may hold values from 256 to 1024, as said below
- out_weight: bfloat16 [2048, 2048], P('tp', 'ep'), may hold values from -0.125 to 0.125
- moe_gain: float32 [2048], replicated, may hold values from 0.1 to 1.9
- route_group: int32 [512], P('ep'), may hold values from 0 to 3, as said below
- route_inner: int32 [512, 2], P('ep'), may hold values from 0 to 31, as said below
- route_weight: bfloat16 [512, 2], P('ep'), may hold values from 0.25 to 1
- gate_w: bfloat16 [128, 2048, 768], P('ep', None, 'tp'), may hold values from -0.125 to 0.125
- up_w: bfloat16 [128, 2048, 768], P('ep', None, 'tp'), may hold values from -0.125 to 0.125
- down_w: bfloat16 [128, 768, 2048], P('ep', 'tp'), may hold values from -0.21875 to 0.21875
Outputs:
- mixed: bfloat16 [512, 2048], P('ep', 'tp')
Inputs may be any that keep to these rules, and one draw needn't show every extreme that they name: `lengths`: some sequence has length 1024 in every draw. Within the rows of one device (aligned blocks of 4 rows) no expert route_group * 32 + route_inner is named twice; one expert is named in every block. `route_inner`: the 2 entries of a row differ.
All inputs are finite; a program needn't handle non-finite values.
Results may differ from a plain program's by a relative error of at most 0.013.
Values may be sent and summed in bfloat16 or wider, within the bound.
A program may use at most 64 MiB of HBM per device.

v0:
```python
import jax
import jax.numpy as jnp
from jax import lax
from jax.sharding import Mesh
from jax.sharding import PartitionSpec as P

EP = ("ep_0", "ep_1", "ep_2")
rms_epsilon = 1e-06


def joined_along(tiles, dim):
    lengths = list(tiles.shape[1:])
    lengths[dim] *= tiles.shape[0]
    return jnp.moveaxis(tiles, 0, dim).reshape(lengths)


def gather_in_order(shard, axes, sequence):
    tiles = shard[None]
    for k in sequence:
        tiles = lax.all_gather(tiles, axes[k], axis=0, tiled=True)
    current = [lax.axis_size(axes[k]) for k in reversed(sequence)]
    tiles = tiles.reshape(*current, *shard.shape)
    turned = sorted(range(len(sequence)), key=lambda place: sequence[len(sequence) - 1 - place])
    return tiles.transpose(*turned, *range(len(sequence), tiles.ndim)).reshape(-1, *shard.shape)


def gathered_by_axis(shard, axes, sequence, dim):
    return joined_along(gather_in_order(shard, axes, sequence), dim)


def in_blocks(shard, dim, peers):
    lengths = shard.shape
    tiles = shard.reshape(*lengths[:dim], peers, lengths[dim] // peers, *lengths[dim + 1 :])
    return jnp.moveaxis(tiles, dim, 0)


def moved_by_axis(tiles, axes, sequence):
    lengths = [lax.axis_size(a) for a in axes]
    tiles = tiles.reshape(*lengths, *tiles.shape[1:])
    for k in sequence:
        tiles = lax.all_to_all(tiles, axes[k], split_axis=k, concat_axis=k, tiled=True)
    return tiles.reshape(-1, *tiles.shape[len(axes) :])


def core_and_chips(shard, groups, sequence, split_dim, concat_dim):
    peers = lax.axis_size(groups[0]) * lax.axis_size(groups[1])
    tiles = in_blocks(shard, split_dim, peers)
    return joined_along(moved_by_axis(tiles, groups, sequence), concat_dim)


def sum_at_owner(shard, axis, dim):
    peers = lax.axis_size(axis)
    tiles = lax.all_to_all(in_blocks(shard, dim, peers), axis, 0, 0, tiled=True)
    return jnp.sum(tiles.astype(jnp.float32), axis=0)


def rms_scale(values, gain):
    wide = values.astype(jnp.float32)
    scaled = wide * lax.rsqrt(jnp.mean(wide * wide, axis=-1, keepdims=True) + rms_epsilon)
    return (scaled * gain).astype(jnp.bfloat16)


def body(
    hidden,
    attn_gain,
    query_weight,
    head_bias,
    key_cache,
    value_cache,
    lengths,
    out_weight,
    moe_gain,
    route_group,
    route_inner,
    route_weight,
    gate_w,
    up_w,
    down_w,
):
    n_tp = lax.axis_size("tp")
    n_ep = lax.axis_size(EP)
    tokens = hidden.shape[0]
    d_model = hidden.shape[1]
    normed = rms_scale(hidden, attn_gain)
    queries = jnp.dot(
        normed, gathered_by_axis(query_weight, EP, (1, 0, 2), 0), preferred_element_type=jnp.float32
    ).astype(jnp.bfloat16)
    head_size = key_cache.shape[3]
    local_kv = key_cache.shape[1]
    cache_len = key_cache.shape[2]
    local_heads = queries.shape[1] // head_size
    group_heads = local_heads // local_kv
    queries = queries.reshape(tokens, local_kv, group_heads, head_size)
    own_bias = lax.dynamic_slice_in_dim(
        head_bias, lax.axis_index("tp") * local_heads, local_heads, 0
    )
    own_bias = own_bias.reshape(local_kv, group_heads)
    scores = jnp.einsum(
        "tkgd,tkpd->tkgp", queries, key_cache, preferred_element_type=jnp.float32
    ) * head_size ** (-0.5)
    scores = scores + own_bias[None, :, :, None]
    position = jnp.arange(cache_len, dtype=jnp.int32)
    visible = position[None, None, None, :] < lengths[:, None, None, None]
    log_keep = jnp.where(visible, jax.nn.log_sigmoid(-scores), 0.0)
    later_sum = lax.cumsum(log_keep, axis=3, reverse=True) - log_keep
    weight = jnp.where(visible, jnp.exp(jax.nn.log_sigmoid(scores) + later_sum), 0.0).astype(
        jnp.bfloat16
    )
    heads_out = jnp.einsum(
        "tkgp,tkpd->tkgd", weight, value_cache, preferred_element_type=jnp.float32
    )
    heads_out = heads_out.astype(jnp.bfloat16).reshape(tokens, -1)
    partial_value = jnp.dot(
        gathered_by_axis(heads_out, EP, (1, 0, 2), 0),
        out_weight,
        preferred_element_type=jnp.float32,
    )
    rounded = lax.optimization_barrier(partial_value.astype(jnp.bfloat16)).astype(jnp.float32)
    col_total = lax.psum(rounded.astype(jnp.bfloat16), "tp").astype(jnp.float32)
    attended = lax.all_to_all(
        col_total.astype(jnp.bfloat16), EP, split_axis=0, concat_axis=1, tiled=True
    ).astype(col_total.dtype)
    residual = (hidden.astype(jnp.float32) + attended).astype(jnp.bfloat16)
    normed_two = rms_scale(residual, moe_gain)
    per_device = gate_w.shape[0]
    experts = per_device * n_ep
    group_count = max(2, experts // 32)
    group_size = experts // group_count
    chosen = route_group[:, None] * group_size + route_inner
    matches = chosen[:, :, None] == jnp.arange(experts, dtype=jnp.int32)[None, None, :]
    picked = jnp.any(matches, axis=1).astype(jnp.bfloat16)
    mixing = jnp.sum(
        jnp.where(matches, route_weight[:, :, None].astype(jnp.float32), 0.0), axis=1
    ).astype(jnp.bfloat16)
    part_width = d_model // n_tp
    own_cols = lax.dynamic_slice_in_dim(
        normed_two, lax.axis_index("tp") * part_width, part_width, 1
    )
    outgoing = jnp.einsum("te,td->ed", picked, own_cols, preferred_element_type=jnp.float32)
    outgoing = outgoing.astype(jnp.bfloat16).reshape(n_ep, per_device, part_width)
    arrived = core_and_chips(outgoing, (("ep_0", "ep_1"), "ep_2"), (1, 0), 0, 0)
    arrived = lax.all_gather(arrived, "tp", axis=2, tiled=True)
    gated_in = jnp.einsum("sed,edf->sef", arrived, gate_w, preferred_element_type=jnp.float32)
    up_proj = jnp.einsum("sed,edf->sef", arrived, up_w, preferred_element_type=jnp.float32)
    activated = (jax.nn.silu(gated_in) * up_proj).astype(jnp.bfloat16)
    down_out = jnp.einsum("sef,efd->sed", activated, down_w, preferred_element_type=jnp.float32)
    down_rounded = lax.optimization_barrier(down_out.astype(jnp.bfloat16)).astype(jnp.float32)
    summed = sum_at_owner(down_rounded.astype(jnp.bfloat16), "tp", 2).astype(jnp.bfloat16)
    returned = lax.all_to_all(summed, EP, split_axis=0, concat_axis=0, tiled=True).reshape(
        experts, part_width
    )
    routed = jnp.dot(mixing, returned, preferred_element_type=jnp.float32)
    own_residual = lax.dynamic_slice_in_dim(
        residual, lax.axis_index("tp") * part_width, part_width, 1
    )
    return (own_residual.astype(jnp.float32) + routed).astype(jnp.bfloat16)


def solution(mesh):
    torus = Mesh(mesh.devices.reshape(16, 4, 2, mesh.shape["tp"]), ("ep_0", "ep_1", "ep_2", "tp"))
    placed = (
        P(EP, None),
        P(),
        P(EP, "tp"),
        P(),
        P(EP, "tp", None, None),
        P(EP, "tp", None, None),
        P(EP),
        P("tp", EP),
        P(),
        P(EP),
        P(EP, None),
        P(EP, None),
        P(EP, None, "tp"),
        P(EP, None, "tp"),
        P(EP, "tp", None),
    )
    return jax.shard_map(body, mesh=torus, in_specs=placed, out_specs=P(EP, "tp"), check_vma=False)
```

profile of v0, /device:TPU:1, one launch (start us, length us, event | category | flops | bytes accessed | tf_op | source)
XLA Modules:
  0.0 320.1 jit_solution(2171377821161092385)
XLA Ops:
  6.5 12.0 %all-gather = bf16[64,512]{1,0:T(8,128)(2,1)} all-gather(bf16[16,512]{1,0:T(8,128)(2,1)} %param.17), channel_id=2, replica_groups=mesh['ep_0'=16,'ep_1'=4,'ep_2'=2,'tp'=4] {'ep_1'}, dimensions={0}, use_global_device_ids=true | all-gather | bytes 81920 | tf_op jit(solution)/shard_map/all_gather | solution.py:20
  18.6 66.4 %all-gather.4.cloned.1.call-done = bf16[64,16,512]{2,1,0:T(8,128)(2,1)} async-done(((bf16[4,16,512]{2,1,0:T(8,128)(2,1)}), bf16[64,16,512]{2,1,0:T(8,128)(2,1)}) %all-gather.4.cloned.1.call-update) | async-done | bytes 1048592 | tf_op jit(solution)/shard_map/all_gather | solution.py:20
  85.0 0.7 dynamic_slice.9
  85.8 0.8 dynamic-slice
  86.5 0.8 fusion.31
  87.4 0.7 broadcast_multiply_fusion
  88.1 0.7 broadcast_add_fusion
  88.7 0.7 iota_compare_fusion
  89.5 27.5 %all-gather.6.cloned.1.call-done = bf16[128,16,512]{2,1,0:T(8,128)(2,1)} async-done(((bf16[64,16,512]{2,1,0:T(8,128)(2,1)}), bf16[128,16,512]{2,1,0:T(8,128)(2,1)}) %all-gather.6.cloned.1.call-update) | async-done | bytes 2097168 | tf_op jit(solution)/shard_map/all_gather | solution.py:20
  117.0 1.8 copy.53
  118.8 0.4 convolution_convert_fusion.4
  119.3 0.4 fusion.29
  119.7 19.8 %reduce-window.6 = f32[4,1,4,8,128]{4,3,2,1,0:T(8,128)S(1)} reduce-window(f32[4,1,4,8,128]{4,3,2,1,0:T(8,128)S(1)} %bitcast.101, f32[]{:T(128)} %constant.9.clone.1), window={size=1x1x1x1x128 pad=0_0x0_0x0_0x0_0x0_127}, to_apply=%region_1.2 | reduce-window | flops 2080768 | bytes 131076 | tf_op jit(solution)/shard_map/reduce-window
  139.7 0.7 reduce-window.9
  141.0 9.1 %all_gather.24 = bf16[4,4,512]{2,1,0:T(4,128)(2,1)S(1)} all-gather(bf16[1,4,512]{2,1,0:T(4,128)(2,1)S(1)} %broadcast_in_dim_reshape.4), channel_id=1, replica_groups=mesh['ep_0'=16,'ep_1'=4,'ep_2'=2,'tp'=4] {'ep_1'}, dimensions={0}, use_global_device_ids=true | all-gather | bytes 20480 | tf_op jit(solution)/shard_map/all_gather | solution.py:20
  150.1 24.1 %all_gather.25 = bf16[64,4,512]{2,1,0:T(4,128)(2,1)S(1)} all-gather(bf16[4,4,512]{2,1,0:T(4,128)(2,1)S(1)} %all_gather.24), channel_id=1, replica_groups=mesh['ep_0'=16,'ep_1'=4,'ep_2'=2,'tp'=4] {'ep_0'}, dimensions={0}, use_global_device_ids=true | all-gather | bytes 278528 | tf_op jit(solution)/shard_map/all_gather | solution.py:20
  174.2 11.7 %all_gather.26 = bf16[128,4,512]{2,1,0:T(4,128)(2,1)S(1)} all-gather(bf16[64,4,512]{2,1,0:T(4,128)(2,1)S(1)} %all_gather.25), channel_id=1, replica_groups=mesh['ep_0'=16,'ep_1'=4,'ep_2'=2,'tp'=4] {'ep_2'}, dimensions={0}, use_global_device_ids=true | all-gather | bytes 786432 | tf_op jit(solution)/shard_map/all_gather | solution.py:20
  186.6 15.2 %psum.7 = bf16[128,4,16]{2,1,0:T(4,128)(2,1)} all-reduce(bf16[128,4,16]{2,1,0:T(4,128)(2,1)S(1)} %bitcast.98), channel_id=1, replica_groups=mesh['ep_0'=16,'ep_1'=4,'ep_2'=2,'tp'=4] {'tp'}, use_global_device_ids=true, to_apply=%region_3.4 | all-reduce | flops 8192 | bytes 32768 | tf_op jit(solution)/shard_map/psum | solution.py:119
  201.8 15.9 %all-to-all-start = ((bf16[128,4,16]{2,1,0:T(4,128)(2,1)}), bf16[128,4,16]{2,1,0:T(4,128)(2,1)S(1)}, u32[]{:S(2)}, u32[]{:S(2)}) async-start(bf16[128,4,16]{2,1,0:T(4,128)(2,1)} %psum.7), calls=%async_computation | async-start | bytes 262144 | tf_op jit(solution)/shard_map/all_to_all | solution.py:120
  217.9 15.9 %all-to-all-done = bf16[128,4,16]{2,1,0:T(4,128)(2,1)S(1)} async-done(((bf16[128,4,16]{2,1,0:T(4,128)(2,1)}), bf16[128,4,16]{2,1,0:T(4,128)(2,1)S(1)}, u32[]{:S(2)}, u32[]{:S(2)}) %all-to-all-start) | async-done | bytes 16416 | tf_op jit(solution)/shard_map/all_to_all | solution.py:120
  234.5 3.9 %all_to_all.33 = bf16[64,2,1,1,512]{4,0,3,2,1:T(8,128)(2,1)S(1)} all-to-all(bf16[64,2,1,1,512]{4,0,3,2,1:T(8,128)(2,1)S(1)} %copy.58), channel_id=1, replica_groups=mesh['ep_0'=16,'ep_1'=4,'ep_2'=2,'tp'=4] {'ep_2'}, dimensions={1} | all-to-all | bytes 262144 | tf_op jit(solution)/shard_map/all_to_all | solution.py:41
  238.5 21.2 %all_to_all.34 = bf16[64,2,1,1,512]{4,1,3,2,0:T(2,128)(2,1)S(1)} all-to-all(bf16[64,2,1,1,512]{4,1,3,2,0:T(2,128)(2,1)S(1)} %copy.59), channel_id=1, replica_groups=mesh['ep_0'=16,'ep_1'=4,'ep_2'=2,'tp'=4] {'ep_0','ep_1'}, dimensions={0} | all-to-all | bytes 262144 | tf_op jit(solution)/shard_map/all_to_all | solution.py:41
  259.8 11.2 %all_gather.27 = bf16[128,1,2048]{2,0,1:T(8,128)(2,1)S(1)} all-gather(bf16[128,1,512]{2,0,1:T(8,128)(2,1)S(1)} %reshape_reshape.11), channel_id=1, replica_groups=mesh['ep_0'=16,'ep_1'=4,'ep_2'=2,'tp'=4] {'tp'}, dimensions={2}, use_global_device_ids=true | all-gather | bytes 655360 | tf_op jit(solution)/shard_map/all_gather | solution.py:142
  271.0 0.4 convolution_bitcast_fusion.1
  271.4 2.1 fusion
  273.5 9.3 %all_to_all.35 = bf16[4,128,1,512]{3,1,2,0:T(8,128)(2,1)S(1)} all-to-all(bf16[4,128,1,512]{3,1,2,0:T(8,128)(2,1)S(1)} %bitcast.96), channel_id=1, replica_groups=mesh['ep_0'=16,'ep_1'=4,'ep_2'=2,'tp'=4] {'tp'}, dimensions={0} | all-to-all | bytes 1048576 | tf_op jit(solution)/shard_map/all_to_all | solution.py:53
  282.9 0.5 broadcast.80
  283.4 0.7 reduce.4
  284.1 0.7 reshape.171
  284.8 11.4 %all-to-all-start.4 = ((bf16[128,2,256]{2,1,0:T(2,128)(2,1)}), bf16[128,2,256]{2,1,0:T(2,128)(2,1)S(1)}, u32[]{:S(2)}, u32[]{:S(2)}) async-start(bf16[128,2,256]{2,1,0:T(2,128)(2,1)} %reshape.171), calls=%async_computation.4 | async-start | bytes 262144 | tf_op jit(solution)/shard_map/all_to_all | solution.py:149
  296.3 16.1 %all-to-all-done.4 = bf16[128,2,256]{2,1,0:T(2,128)(2,1)S(1)} async-done(((bf16[128,2,256]{2,1,0:T(2,128)(2,1)}), bf16[128,2,256]{2,1,0:T(2,128)(2,1)S(1)}, u32[]{:S(2)}, u32[]{:S(2)}) %all-to-all-start.4) | async-done | bytes 131104 | tf_op jit(solution)/shard_map/all_to_all | solution.py:149
  312.5 0.7 fusion.5
  (51 shorter events, 2.8 us)
Async XLA Ops:
  6.5 112.7 %copy-start = (bf16[4,1,1024,128]{3,2,1,0:T(8,128)(2,1)S(1)}, bf16[4,1,1024,128]{3,2,1,0:T(8,128)(2,1)}, u32[]{:S(2)}) copy-start(bf16[4,1,1024,128]{3,2,1,0:T(8,128)(2,1)} %param.19) | copy-start | bytes 3145732
  6.5 78.5 %all-gather.4.cloned.1.call-start = ((), (), s32[]{:S(2)}) async-start(), calls=%async_computation.5 | async-start | bytes 1114112 | tf_op jit(solution)/shard_map/all_gather | solution.py:20
  18.6 98.4 %all-gather.6.cloned.1.call-start = ((), (), s32[]{:S(2)}) async-start(), calls=%async_computation.6 | async-start | bytes 3145728 | tf_op jit(solution)/shard_map/all_gather | solution.py:20
  117.0 1.8 copy-start.3
  117.0 1.9 copy-start.5
  118.8 21.8 %copy-start.6 = (bf16[4,1,1024,128]{3,2,1,0:T(8,128)(2,1)S(1)}, bf16[4,1,1024,128]{3,2,1,0:T(8,128)(2,1)}, u32[]{:S(2)}) copy-start(bf16[4,1,1024,128]{3,2,1,0:T(8,128)(2,1)} %param.20) | copy-start | bytes 3145732
  140.6 45.6 %copy-start.4 = (bf16[512,16]{0,1:T(8,128)(2,1)S(1)}, bf16[512,16]{0,1:T(8,128)(2,1)}, u32[]{:S(2)}) copy-start(bf16[512,16]{0,1:T(8,128)(2,1)} %param.22) | copy-start | bytes 49156
  186.6 84.4 %copy-start.1 = (bf16[1,2048,192]{1,2,0:T(8,128)(2,1)S(1)}, bf16[1,2048,192]{1,2,0:T(8,128)(2,1)}, u32[]{:S(2)}) copy-start(bf16[1,2048,192]{1,2,0:T(8,128)(2,1)} %param.27) | copy-start | bytes 2359300
  201.8 31.9 %all-to-all-start = ((bf16[128,4,16]{2,1,0:T(4,128)(2,1)}), bf16[128,4,16]{2,1,0:T(4,128)(2,1)S(1)}, u32[]{:S(2)}, u32[]{:S(2)}) async-start(bf16[128,4,16]{2,1,0:T(4,128)(2,1)} %psum.7), calls=%async_computation | async-start | bytes 262144 | tf_op jit(solution)/shard_map/all_to_all | solution.py:120
  233.8 37.6 %copy-start.2 = (bf16[1,192,2048]{2,1,0:T(8,128)(2,1)S(1)}, bf16[1,192,2048]{2,1,0:T(8,128)(2,1)}, u32[]{:S(2)}) copy-start(bf16[1,192,2048]{2,1,0:T(8,128)(2,1)} %param.29) | copy-start | bytes 2359300
  273.5 22.8 %copy-start.7 = (bf16[4,2]{0,1:T(2,128)(2,1)S(1)}, bf16[4,2]{0,1:T(2,128)(2,1)}, u32[]{:S(2)}) copy-start(bf16[4,2]{0,1:T(2,128)(2,1)} %param.26) | copy-start | bytes 52
  284.8 27.6 %all-to-all-start.4 = ((bf16[128,2,256]{2,1,0:T(2,128)(2,1)}), bf16[128,2,256]{2,1,0:T(2,128)(2,1)S(1)}, u32[]{:S(2)}, u32[]{:S(2)}) async-start(bf16[128,2,256]{2,1,0:T(2,128)(2,1)} %reshape.171), calls=%async_computation.4 | async-start | bytes 262144 | tf_op jit(solution)/shard_map/all_to_all | solution.py:149
Sparse Core Ops, SparseCore 0:
  18.7 66.2 all-gather.3
  87.1 29.8 all-gather.5
where the time goes:
time: 321 us; the launch traced here: 320 us
  waiting for transfers between devices  126 us (39%)
  blocking collectives  118 us (37%)
  starting transfers between devices  27.4 us (9%)
  other arithmetic  24.6 us (8%)
  between operations  13.7 us (4%)
  local copies, waits for them, and re-layouts  5.95 us (2%)
  matrix products  4.82 us (2%)
    all_gather x2, waiting for transfers between devices, gather_in_order(): tiles = lax.all_gather(tiles, axes[k], axis=0, tiled=True)  93.9 us
    all_gather x4, blocking collectives, gather_in_order(): tiles = lax.all_gather(tiles, axes[k], axis=0, tiled=True)  56.9 us
    all_to_all x2, blocking collectives, moved_by_axis(): lax.all_to_all(tiles, axes[k], split_axis=k, concat_axis=k, tiled=True)  25.1 us
    another operation x2, other arithmetic  20.5 us
    all_to_all x1, waiting for transfers between devices, body(): lax.all_to_all(summed, EP, split_axis=0, concat_axis=0, tiled=True)  16.1 us
    all_to_all x1, starting transfers between devices, body(): lax.all_to_all(col_total.astype(jnp.bfloat16), EP, split_axis=0, concat_a...  15.9 us
    all_to_all x1, waiting for transfers between devices, body(): lax.all_to_all(col_total.astype(jnp.bfloat16), EP, split_axis=0, concat_a...  15.9 us
    psum x1, blocking collectives, body(): col_total = lax.psum(rounded.astype(jnp.bfloat16), 'tp').astype(jnp.float32)  15.2 us
  transfers between devices with their start and end apart: 4, of which 4 were waited for; matrix products, arithmetic and copies ran while one was open for 1% of the time, Pallas kernels for 0%

commit v1 on v0

--- a/solution.py
+++ b/solution.py
@@ -17,7 +17,8 @@
 def gather_in_order(shard, axes, sequence):
     tiles = shard[None]
     for k in sequence:
-        tiles = lax.all_gather(tiles, axes[k], axis=0, tiled=True)
+        stack = jnp.stack([tiles] * lax.axis_size(axes[k]))
+        tiles = jnp.concatenate(lax.all_to_all(stack, axes[k], 0, 0), axis=0)
     current = [lax.axis_size(axes[k]) for k in reversed(sequence)]
     tiles = tiles.reshape(*current, *shard.shape)
     turned = sorted(range(len(sequence)), key=lambda place: sequence[len(sequence) - 1 - place])

time: 321 us -> 268 us (0.83)
  waiting for transfers between devices: 126 us -> 88.2 us
  blocking collectives: 118 us -> 98.2 us
  starting transfers between devices: 27.4 us -> 46 us
  between operations: 13.7 us -> 0.35 us
    all_gather x2 -> x0, waiting for transfers between devices: 93.9 us -> none  [gather_in_order(): tiles = lax.all_gather(tiles, axes[k], axis=0, tiled=True)]
    all_gather x4 -> x0, blocking collectives: 56.9 us -> none  [gather_in_order(): tiles = lax.all_gather(tiles, axes[k], axis=0, tiled=True)]
    all_to_all x0 -> x2, waiting for transfers between devices: none -> 56.2 us  [gather_in_order(): tiles = jnp.concatenate(lax.all_to_all(stack, axes[k], 0, 0), axis=0)]
    all_to_all x0 -> x4, blocking collectives: none -> 37.1 us  [gather_in_order(): tiles = jnp.concatenate(lax.all_to_all(stack, axes[k], 0, 0), axis=0)]
    all_to_all x0 -> x2, starting transfers between devices: none -> 23.1 us  [gather_in_order(): tiles = jnp.concatenate(lax.all_to_all(stack, axes[k], 0, 0), axis=0)]
    all_to_all x1, starting transfers between devices: 15.9 us -> 11.5 us  [body(): lax.all_to_all(col_total.astype(jnp.bfloat16), EP, split_axis=0, concat_a...]
    another operation x2 -> x4, other arithmetic: 20.5 us -> 21 us
  transfers between devices with their start and end apart: 4 -> 4, of which waited for: 4 -> 4; matrix products, arithmetic and copies ran while one was open for 1% -> 0% of each run, Pallas kernels for 0% -> 0%
where the time goes in v1:
time: 268 us; the launch traced here: 267 us
  blocking collectives  98.2 us (37%)
  waiting for transfers between devices  88.2 us (33%)
  starting transfers between devices  46 us (17%)
  other arithmetic  22.3 us (8%)
  local copies, waits for them, and re-layouts  6.91 us (3%)
  matrix products  4.82 us (2%)
    all_to_all x2, waiting for transfers between devices, gather_in_order(): tiles = jnp.concatenate(lax.all_to_all(stack, axes[k], 0, 0), axis=0)  56.2 us
    all_to_all x4, blocking collectives, gather_in_order(): tiles = jnp.concatenate(lax.all_to_all(stack, axes[k], 0, 0), axis=0)  37.1 us
    all_to_all x2, blocking collectives, moved_by_axis(): lax.all_to_all(tiles, axes[k], split_axis=k, concat_axis=k, tiled=True)  25.1 us
    all_to_all x2, starting transfers between devices, gather_in_order(): tiles = jnp.concatenate(lax.all_to_all(stack, axes[k], 0, 0), axis=0)  23.1 us
    another operation x2, other arithmetic  20.5 us
    all_to_all x1, waiting for transfers between devices, body(): lax.all_to_all(summed, EP, split_axis=0, concat_axis=0, tiled=True)  16.1 us
    all_to_all x1, waiting for transfers between devices, body(): lax.all_to_all(col_total.astype(jnp.bfloat16), EP, split_axis=0, concat_a...  15.9 us
    psum x1, blocking collectives, body(): col_total = lax.psum(rounded.astype(jnp.bfloat16), 'tp').astype(jnp.float32)  15.5 us
  transfers between devices with their start and end apart: 4, of which 4 were waited for; matrix products, arithmetic and copies ran while one was open for 0% of the time, Pallas kernels for 0%

profile of v1, /device:TPU:1, one launch (start us, length us, event | category | flops | bytes accessed | tf_op | source)
XLA Modules:
  0.0 266.8 jit_solution(1854134920195677448)
XLA Ops:
  0.0 0.8 stack.18
  0.8 9.1 %all_to_all.63 = bf16[4,1,16,512]{3,2,1,0:T(8,128)(2,1)S(1)} all-to-all(bf16[4,1,16,512]{3,2,1,0:T(8,128)(2,1)S(1)} %stack.18), channel_id=1, replica_groups=mesh['ep_0'=16,'ep_1'=4,'ep_2'=2,'tp'=4] {'ep_1'}, dimensions={0} | all-to-all | bytes 131072 | tf_op jit(solution)/shard_map/all_to_all | solution.py:21
  9.9 1.1 stack.19
  11.0 14.9 %all-to-all-start.1 = ((bf16[16,4,16,512]{3,2,1,0:T(8,128)(2,1)}), bf16[16,4,16,512]{3,2,1,0:T(8,128)(2,1)S(1)}, u32[]{:S(2)}, u32[]{:S(2)}) async-start(bf16[16,4,16,512]{3,2,1,0:T(8,128)(2,1)} %stack.19), calls=%async_computation.1 | async-start | bytes 2097152 | tf_op jit(solution)/shard_map/all_to_all | solution.py:21
  26.3 44.3 %all-to-all-done.1 = bf16[16,4,16,512]{3,2,1,0:T(8,128)(2,1)S(1)} async-done(((bf16[16,4,16,512]{3,2,1,0:T(8,128)(2,1)}), bf16[16,4,16,512]{3,2,1,0:T(8,128)(2,1)S(1)}, u32[]{:S(2)}, u32[]{:S(2)}) %all-to-all-start.1) | async-done | bytes 1048608 | tf_op jit(solution)/shard_map/all_to_all | solution.py:21
  70.8 10.6 %all_to_all.64 = bf16[2,64,16,512]{3,2,1,0:T(8,128)(2,1)S(1)} all-to-all(bf16[2,64,16,512]{3,2,1,0:T(8,128)(2,1)S(1)} %pad_maximum_fusion), channel_id=1, replica_groups=mesh['ep_0'=16,'ep_1'=4,'ep_2'=2,'tp'=4] {'ep_2'}, dimensions={0} | all-to-all | bytes 4194304 | tf_op jit(solution)/shard_map/all_to_all | solution.py:21
  81.6 0.4 copy-done.5
  82.0 0.4 convolution_convert_fusion.4
  82.5 0.4 fusion.30
  82.9 19.8 %reduce-window.6 = f32[4,1,4,8,128]{4,3,2,1,0:T(8,128)S(1)} reduce-window(f32[4,1,4,8,128]{4,3,2,1,0:T(8,128)S(1)} %bitcast.113, f32[]{:T(128)} %constant.9.clone.1), window={size=1x1x1x1x128 pad=0_0x0_0x0_0x0_0x0_127}, to_apply=%region_1.2 | reduce-window | flops 2080768 | bytes 131076 | tf_op jit(solution)/shard_map/reduce-window
  102.9 0.7 reduce-window.9
  103.8 0.4 fusion.6
  104.2 6.7 %all_to_all.65 = bf16[4,1,4,512]{3,2,1,0:T(4,128)(2,1)S(1)} all-to-all(bf16[4,1,4,512]{3,2,1,0:T(4,128)(2,1)S(1)} %stack.21), channel_id=1, replica_groups=mesh['ep_0'=16,'ep_1'=4,'ep_2'=2,'tp'=4] {'ep_1'}, dimensions={0} | all-to-all | bytes 32768 | tf_op jit(solution)/shard_map/all_to_all | solution.py:21
  111.0 0.8 stack.22
  111.8 8.2 %all-to-all-start.4 = ((bf16[16,4,4,512]{3,2,1,0:T(4,128)(2,1)}), bf16[16,4,4,512]{3,2,1,0:T(4,128)(2,1)S(1)}, u32[]{:S(2)}, u32[]{:S(2)}) async-start(bf16[16,4,4,512]{3,2,1,0:T(4,128)(2,1)} %stack.22), calls=%async_computation.4 | async-start | bytes 524288 | tf_op jit(solution)/shard_map/all_to_all | solution.py:21
  120.0 0.8 dynamic-slice
  120.8 11.9 %all-to-all-done.4 = bf16[16,4,4,512]{3,2,1,0:T(4,128)(2,1)S(1)} async-done(((bf16[16,4,4,512]{3,2,1,0:T(4,128)(2,1)}), bf16[16,4,4,512]{3,2,1,0:T(4,128)(2,1)S(1)}, u32[]{:S(2)}, u32[]{:S(2)}) %all-to-all-start.4) | async-done | bytes 262176 | tf_op jit(solution)/shard_map/all_to_all | solution.py:21
  133.0 10.7 %all_to_all.66 = bf16[2,64,4,512]{3,2,1,0:T(4,128)(2,1)S(1)} all-to-all(bf16[2,64,4,512]{3,2,1,0:T(4,128)(2,1)S(1)} %pad_maximum_fusion.1), channel_id=1, replica_groups=mesh['ep_0'=16,'ep_1'=4,'ep_2'=2,'tp'=4] {'ep_2'}, dimensions={0} | all-to-all | bytes 1048576 | tf_op jit(solution)/shard_map/all_to_all | solution.py:21
  144.4 15.5 %psum.7 = bf16[128,4,16]{2,1,0:T(4,128)(2,1)} all-reduce(bf16[128,4,16]{2,1,0:T(4,128)(2,1)S(1)} %bitcast.110), channel_id=1, replica_groups=mesh['ep_0'=16,'ep_1'=4,'ep_2'=2,'tp'=4] {'tp'}, use_global_device_ids=true, to_apply=%region_3.4 | all-reduce | flops 8192 | bytes 32768 | tf_op jit(solution)/shard_map/psum | solution.py:120
  159.9 11.5 %all-to-all-start.6 = ((bf16[128,4,16]{2,1,0:T(4,128)(2,1)}), bf16[128,4,16]{2,1,0:T(4,128)(2,1)S(1)}, u32[]{:S(2)}, u32[]{:S(2)}) async-start(bf16[128,4,16]{2,1,0:T(4,128)(2,1)} %psum.7), calls=%async_computation.6 | async-start | bytes 262144 | tf_op jit(solution)/shard_map/all_to_all | solution.py:121
  171.4 15.9 %all-to-all-done.6 = bf16[128,4,16]{2,1,0:T(4,128)(2,1)S(1)} async-done(((bf16[128,4,16]{2,1,0:T(4,128)(2,1)}), bf16[128,4,16]{2,1,0:T(4,128)(2,1)S(1)}, u32[]{:S(2)}, u32[]{:S(2)}) %all-to-all-start.6) | async-done | bytes 16416 | tf_op jit(solution)/shard_map/all_to_all | solution.py:121
  188.0 3.9 %all_to_all.67 = bf16[64,2,1,1,512]{4,0,3,2,1:T(8,128)(2,1)S(1)} all-to-all(bf16[64,2,1,1,512]{4,0,3,2,1:T(8,128)(2,1)S(1)} %copy.51), channel_id=1, replica_groups=mesh['ep_0'=16,'ep_1'=4,'ep_2'=2,'tp'=4] {'ep_2'}, dimensions={1} | all-to-all | bytes 262144 | tf_op jit(solution)/shard_map/all_to_all | solution.py:42
  192.1 21.2 %all_to_all.68 = bf16[64,2,1,1,512]{4,1,3,2,0:T(2,128)(2,1)S(1)} all-to-all(bf16[64,2,1,1,512]{4,1,3,2,0:T(2,128)(2,1)S(1)} %copy.52), channel_id=1, replica_groups=mesh['ep_0'=16,'ep_1'=4,'ep_2'=2,'tp'=4] {'ep_0','ep_1'}, dimensions={0} | all-to-all | bytes 262144 | tf_op jit(solution)/shard_map/all_to_all | solution.py:42
  213.3 11.2 %all_gather.3 = bf16[128,1,2048]{2,0,1:T(8,128)(2,1)S(1)} all-gather(bf16[128,1,512]{2,0,1:T(8,128)(2,1)S(1)} %reshape_reshape.19), channel_id=1, replica_groups=mesh['ep_0'=16,'ep_1'=4,'ep_2'=2,'tp'=4] {'tp'}, dimensions={2}, use_global_device_ids=true | all-gather | bytes 655360 | tf_op jit(solution)/shard_map/all_gather | solution.py:143
  224.9 2.1 fusion
  227.1 9.3 %all_to_all.69 = bf16[4,128,1,512]{3,1,2,0:T(8,128)(2,1)S(1)} all-to-all(bf16[4,128,1,512]{3,1,2,0:T(8,128)(2,1)S(1)} %bitcast.107), channel_id=1, replica_groups=mesh['ep_0'=16,'ep_1'=4,'ep_2'=2,'tp'=4] {'tp'}, dimensions={0} | all-to-all | bytes 1048576 | tf_op jit(solution)/shard_map/all_to_all | solution.py:54
  236.5 0.5 broadcast.86
  237.0 0.7 reduce.4
  237.7 0.7 reshape.172
  238.4 11.4 %all-to-all-start.10 = ((bf16[128,2,256]{2,1,0:T(2,128)(2,1)}), bf16[128,2,256]{2,1,0:T(2,128)(2,1)S(1)}, u32[]{:S(2)}, u32[]{:S(2)}) async-start(bf16[128,2,256]{2,1,0:T(2,128)(2,1)} %reshape.172), calls=%async_computation.10 | async-start | bytes 262144 | tf_op jit(solution)/shard_map/all_to_all | solution.py:150
  249.9 16.1 %all-to-all-done.10 = bf16[128,2,256]{2,1,0:T(2,128)(2,1)S(1)} async-done(((bf16[128,2,256]{2,1,0:T(2,128)(2,1)}), bf16[128,2,256]{2,1,0:T(2,128)(2,1)S(1)}, u32[]{:S(2)}, u32[]{:S(2)}) %all-to-all-start.10) | async-done | bytes 131104 | tf_op jit(solution)/shard_map/all_to_all | solution.py:150
  266.0 0.7 fusion.5
  (63 shorter events, 3.7 us)
Async XLA Ops:
  0.0 82.5 %copy-start = (bf16[4,1,1024,128]{3,2,1,0:T(8,128)(2,1)S(1)}, bf16[4,1,1024,128]{3,2,1,0:T(8,128)(2,1)}, u32[]{:S(2)}) copy-start(bf16[4,1,1024,128]{3,2,1,0:T(8,128)(2,1)} %param.19) | copy-start | bytes 3145732
  0.0 26.0 %copy-start.9 = (f32[16]{0:T(128)S(1)}, f32[16]{0:T(128)}, u32[]{:S(2)}) copy-start(f32[16]{0:T(128)} %param.18) | copy-start | bytes 196
  0.0 26.1 %copy-start.3 = (bf16[4,2048]{1,0:T(4,128)(2,1)S(1)}, bf16[4,2048]{1,0:T(4,128)(2,1)}, u32[]{:S(2)}) copy-start(bf16[4,2048]{1,0:T(4,128)(2,1)} %param.15) | copy-start | bytes 49156
  0.0 26.2 %copy-start.7 = (s32[4]{0:T(128)S(1)}, s32[4]{0:T(128)}, u32[]{:S(2)}) copy-start(s32[4]{0:T(128)} %param.21) | copy-start | bytes 52
  11.0 59.5 %all-to-all-start.1 = ((bf16[16,4,16,512]{3,2,1,0:T(8,128)(2,1)}), bf16[16,4,16,512]{3,2,1,0:T(8,128)(2,1)S(1)}, u32[]{:S(2)}, u32[]{:S(2)}) async-start(bf16[16,4,16,512]{3,2,1,0:T(8,128)(2,1)} %stack.19), calls=%async_computation.1 | async-start | bytes 2097152 | tf_op jit(solution)/shard_map/all_to_all | solution.py:21
  81.3 0.7 copy-start.5
  81.6 22.2 %copy-start.8 = (bf16[4,1,1024,128]{3,2,1,0:T(8,128)(2,1)S(1)}, bf16[4,1,1024,128]{3,2,1,0:T(8,128)(2,1)}, u32[]{:S(2)}) copy-start(bf16[4,1,1024,128]{3,2,1,0:T(8,128)(2,1)} %param.20) | copy-start | bytes 3145732
  82.5 38.3 %copy-start.10 = (s32[4]{0:T(128)S(1)}, s32[4]{0:T(128)}, u32[]{:S(2)}) copy-start(s32[4]{0:T(128)} %param.24) | copy-start | bytes 52
  82.5 38.3 %copy-start.6 = (s32[4,2]{0,1:T(2,128)S(1)}, s32[4,2]{0,1:T(2,128)}, u32[]{:S(2)}) copy-start(s32[4,2]{0,1:T(2,128)} %param.25) | copy-start | bytes 100
  111.8 20.9 %all-to-all-start.4 = ((bf16[16,4,4,512]{3,2,1,0:T(4,128)(2,1)}), bf16[16,4,4,512]{3,2,1,0:T(4,128)(2,1)S(1)}, u32[]{:S(2)}, u32[]{:S(2)}) async-start(bf16[16,4,4,512]{3,2,1,0:T(4,128)(2,1)} %stack.22), calls=%async_computation.4 | async-start | bytes 524288 | tf_op jit(solution)/shard_map/all_to_all | solution.py:21
  120.0 24.0 %copy-start.4 = (bf16[512,16]{0,1:T(8,128)(2,1)S(1)}, bf16[512,16]{0,1:T(8,128)(2,1)}, u32[]{:S(2)}) copy-start(bf16[512,16]{0,1:T(8,128)(2,1)} %param.22) | copy-start | bytes 49156
  144.4 80.2 %copy-start.1 = (bf16[1,2048,192]{1,2,0:T(8,128)(2,1)S(1)}, bf16[1,2048,192]{1,2,0:T(8,128)(2,1)}, u32[]{:S(2)}) copy-start(bf16[1,2048,192]{1,2,0:T(8,128)(2,1)} %param.27) | copy-start | bytes 2359300
  159.9 27.5 %all-to-all-start.6 = ((bf16[128,4,16]{2,1,0:T(4,128)(2,1)}), bf16[128,4,16]{2,1,0:T(4,128)(2,1)S(1)}, u32[]{:S(2)}, u32[]{:S(2)}) async-start(bf16[128,4,16]{2,1,0:T(4,128)(2,1)} %psum.7), calls=%async_computation.6 | async-start | bytes 262144 | tf_op jit(solution)/shard_map/all_to_all | solution.py:121
  187.4 37.6 %copy-start.2 = (bf16[1,192,2048]{2,1,0:T(8,128)(2,1)S(1)}, bf16[1,192,2048]{2,1,0:T(8,128)(2,1)}, u32[]{:S(2)}) copy-start(bf16[1,192,2048]{2,1,0:T(8,128)(2,1)} %param.29) | copy-start | bytes 2359300
  227.0 22.8 %copy-start.11 = (bf16[4,2]{0,1:T(2,128)(2,1)S(1)}, bf16[4,2]{0,1:T(2,128)(2,1)}, u32[]{:S(2)}) copy-start(bf16[4,2]{0,1:T(2,128)(2,1)} %param.26) | copy-start | bytes 52
  238.4 27.6 %all-to-all-start.10 = ((bf16[128,2,256]{2,1,0:T(2,128)(2,1)}), bf16[128,2,256]{2,1,0:T(2,128)(2,1)S(1)}, u32[]{:S(2)}, u32[]{:S(2)}) async-start(bf16[128,2,256]{2,1,0:T(2,128)(2,1)} %reshape.172), calls=%async_computation.10 | async-start | bytes 262144 | tf_op jit(solution)/shard_map/all_to_all | solution.py:150
